TPU v7x, 512 devices: a 8x2x16 block of a 8x8x16 slice. The times are simulated.
512 devices in a mesh: grp: 2 (over y), sp: 16 (over z), dp: 16 (over x, core).
Axes of the slice: x: 8, y: 2, z: 16, core: 2. Of those that a mesh axis runs over, the one named last changes fastest.
The devices are a block of a 8x8x16 slice.
Arguments:
- tokens: bfloat16 [32, 2048, 2048], P(('grp', 'dp'), 'sp'), parts along dimension 0, may hold values from -6 to 6
- forget_offset: float32 [32, 2048], P(('grp', 'dp'), 'sp'), parts along dimension 0, may hold values from -1.2 to 1.2, as said below
- q_weight: bfloat16 [2048, 2048], P(None, 'dp'), may hold values from -0.125 to 0.125
- k_weight: bfloat16 [2048, 512], P(None, 'dp'), may hold values from -0.125 to 0.125
- v_weight: bfloat16 [2048, 512], P(None, 'dp'), may hold values from -0.125 to 0.125
- forget_weight: bfloat16 [2048, 16], replicated, may hold values from -0.125 to 0.125
- forget_bias: float32 [16], replicated, may hold values from 3 to 12
- score_gain: float32 [16], replicated, may hold values from 0.5 to 80
- out_gain: float32 [2048], replicated, may hold values from 0.1 to 1.9
Outputs:
- attended: bfloat16 [32, 2048, 2048], P(('grp', 'dp'), 'sp'), parts along dimension 0
There are 2 independent parts, one for each index of `grp`. A program takes and returns all parts, laid end to end along the dimension named above; an argument that names none is the same for every part. Nothing has to cross between parts.
Inputs may be any that keep to these rules, and one draw needn't show every extreme that they name: `forget_offset`: constant over aligned spans of 64 positions.
All inputs are finite; a program needn't handle non-finite values.
Results may differ from a plain program's by a relative error of at most 0.0085.
The roundings to bfloat16 on the way count: a program that leaves them out, or rounds other values in their place, can miss the bound.
Values may be sent and summed in bfloat16 or wider, within the bound.
No kernel may reach another device: no remote copies, remote signals or barrier semaphores. Data moves between devices by JAX's collectives and lax.ppermute only.
A program may use at most 128 MiB of HBM per device.

v0:
```python
import jax
import jax.numpy as jnp
from jax import lax
from jax.sharding import PartitionSpec as P

NEG = -1e30
QK_FLOOR = 0.1
OUT_FLOOR = 0.001


def turned_gather(arrays, axis, dims):
    turned = [jnp.moveaxis(a, dim, 0) for a, dim in zip(arrays, dims)]
    both = jnp.concatenate([t.reshape(len(t), -1) for t in turned], axis=1)
    whole, at, done = (lax.all_gather(both, axis, axis=0, tiled=True), 0, [])
    for t, dim in zip(turned, dims):
        piece = whole[:, at : at + t[0].size].reshape(-1, *t.shape[1:])
        done.append(jnp.moveaxis(piece, 0, dim))
        at += t[0].size
    return tuple(done)


def head_norm(vectors, floor):
    return vectors * lax.rsqrt(jnp.mean(vectors * vectors, axis=-1, keepdims=True) + floor)


def local(
    tokens,
    forget_offset,
    q_weight,
    k_weight,
    v_weight,
    forget_weight,
    forget_bias,
    score_gain,
    out_gain,
):
    own_rows = tokens[0]
    tok_count = own_rows.shape[0]
    head_count = forget_bias.shape[0]
    head_dim = out_gain.shape[0] // head_count
    kv_heads = k_weight.shape[1] * lax.axis_size("dp") // head_dim
    spread = lax.axis_size("sp")
    local_heads = head_count // spread
    local_kv = max(1, kv_heads // spread)
    group_size = local_heads // local_kv
    queries = jnp.dot(
        own_rows,
        lax.all_gather(q_weight, "dp", axis=1, tiled=True),
        preferred_element_type=jnp.float32,
    ).astype(jnp.bfloat16)
    key_full, value_full = turned_gather((k_weight, v_weight), "dp", (1, 1))
    keys_proj = jnp.dot(own_rows, key_full, preferred_element_type=jnp.float32).astype(jnp.bfloat16)
    values_proj = jnp.dot(own_rows, value_full, preferred_element_type=jnp.float32).astype(
        jnp.bfloat16
    )
    forget_input = (
        jnp.dot(own_rows, forget_weight, preferred_element_type=jnp.float32)
        + forget_offset[0][:, None]
    ).astype(jnp.bfloat16)
    query_send = queries.reshape(tok_count, spread, local_heads, head_dim)
    forget_send = forget_input.reshape(tok_count, spread, local_heads)
    copies = spread // kv_heads
    key_send = jnp.broadcast_to(
        keys_proj.reshape(tok_count, kv_heads, 1, head_dim), (tok_count, kv_heads, copies, head_dim)
    ).reshape(tok_count, spread, 1, head_dim)
    value_send = jnp.broadcast_to(
        values_proj.reshape(tok_count, kv_heads, 1, head_dim),
        (tok_count, kv_heads, copies, head_dim),
    ).reshape(tok_count, spread, 1, head_dim)
    query_head, forget_head, key_head, value_head = (
        lax.all_to_all(query_send, "sp", split_axis=1, concat_axis=0, tiled=True),
        lax.all_to_all(forget_send, "sp", split_axis=1, concat_axis=0, tiled=True),
        lax.all_to_all(key_send, "sp", split_axis=1, concat_axis=0, tiled=True),
        lax.all_to_all(value_send, "sp", split_axis=1, concat_axis=0, tiled=True),
    )
    length = query_head.shape[0]
    first_head = lax.axis_index("sp") * local_heads
    bias_local = lax.dynamic_slice_in_dim(forget_bias, first_head, local_heads, 0)
    gain_local = lax.dynamic_slice_in_dim(score_gain, first_head, local_heads, 0)
    norm_local = lax.dynamic_slice_in_dim(
        out_gain, first_head * head_dim, local_heads * head_dim, 0
    )
    log_gate = jax.nn.log_sigmoid(
        forget_head.reshape(length, local_heads).astype(jnp.float32) + bias_local[None, :]
    )
    cumulative = jnp.cumsum(log_gate, axis=0).reshape(length, local_kv, group_size)
    query_unit = head_norm(query_head.astype(jnp.float32), QK_FLOOR).astype(jnp.bfloat16)
    key_unit = head_norm(
        key_head.reshape(length, local_kv, head_dim).astype(jnp.float32), QK_FLOOR
    ).astype(jnp.bfloat16)
    value_heads = value_head.reshape(length, local_kv, head_dim)
    factor = (gain_local * head_dim ** (-0.5)).reshape(local_kv, group_size)
    out_gains = norm_local.reshape(local_kv, group_size, head_dim)
    key_totals = jnp.transpose(cumulative, (1, 2, 0))
    span_rows = 512
    positions = jnp.arange(length, dtype=jnp.int32)

    def attend_block(block_index):
        first = block_index * span_rows
        query_block = lax.dynamic_slice_in_dim(query_unit, first, span_rows, 0)
        query_totals = lax.dynamic_slice_in_dim(cumulative, first, span_rows, 0)
        scores = jnp.einsum(
            "qkgd,skd->kgqs", query_block, key_unit, preferred_element_type=jnp.float32
        )
        scores = (
            scores * factor[:, :, None, None]
            + jnp.transpose(query_totals, (1, 2, 0))[..., None]
            - key_totals[:, :, None, :]
        )
        allowed = positions[None, :] <= (first + jnp.arange(span_rows, dtype=jnp.int32))[:, None]
        scores = jnp.where(allowed[None, None], scores, NEG)
        row_peak = jnp.max(scores, axis=-1, keepdims=True)
        exponent = jnp.exp(scores - row_peak)
        weights = (exponent / jnp.sum(exponent, axis=-1, keepdims=True)).astype(jnp.bfloat16)
        mixed = jnp.einsum(
            "kgqs,skd->qkgd", weights, value_heads, preferred_element_type=jnp.float32
        )
        return (head_norm(mixed, OUT_FLOOR) * out_gains).astype(jnp.bfloat16)

    outputs = lax.map(attend_block, jnp.arange(length // span_rows, dtype=jnp.int32))
    outputs = outputs.reshape(length, local_heads, head_dim)
    back_rows = lax.all_to_all(outputs, "sp", split_axis=0, concat_axis=1, tiled=True)
    return back_rows.reshape(1, tok_count, head_count * head_dim)


def solution(mesh):
    in_specs = (
        P(("grp", "dp"), "sp", None),
        P(("grp", "dp"), "sp"),
        P(None, "dp"),
        P(None, "dp"),
        P(None, "dp"),
        P(),
        P(),
        P(),
        P(),
    )
    out_specs = P(("grp", "dp"), "sp", None)
    return jax.shard_map(local, mesh=mesh, in_specs=in_specs, out_specs=out_specs, check_vma=False)
```

profile of v0, /device:TPU:66, one launch (start us, length us, event | category | flops | bytes accessed | tf_op | source)
XLA Modules:
  0.0 312.4 jit_solution(6039166641499261542)
XLA Ops:
  6.6 1.7 pad_maximum_fusion
  8.4 0.7 all-gather.3.cloned.1.call-update
  9.2 1.1 fusion.29
  10.9 43.7 %all-to-all-start.2 = ((bf16[128,16,1]{0,2,1:T(2,128)(2,1)}), bf16[128,16,1]{0,2,1:T(2,128)(2,1)S(1)}, u32[]{:S(2)}, u32[]{:S(2)}) async-start(bf16[128,16,1]{0,2,1:T(2,128)(2,1)} %copy.52), calls=%async_computation.2 | async-start | bytes 16384 | tf_op jit(solution)/shard_map/all_to_all | solution.py:72
  54.6 36.7 %all-gather.5.cloned.1.call-done = bf16[512,4096]{1,0:T(8,128)(2,1)} async-done(((bf16[32,4096]{1,0:T(8,128)(2,1)}), bf16[512,4096]{1,0:T(8,128)(2,1)}) %all-gather.5.cloned.1.call-update) | async-done | bytes 4194320 | tf_op jit(solution)/shard_map/all_gather | solution.py:14
  91.2 2.3 fusion.22
  93.7 0.9 broadcast_in_dim.36
  94.6 13.1 %all-to-all-start.1 = ((bf16[128,16,1,128]{3,0,2,1:T(8,128)(2,1)}), bf16[128,16,1,128]{3,0,2,1:T(8,128)(2,1)S(1)}, u32[]{:S(2)}, u32[]{:S(2)}) async-start(bf16[128,16,1,128]{3,0,2,1:T(8,128)(2,1)} %bitcast.10), calls=%async_computation.1 | async-start | bytes 1048576 | tf_op jit(solution)/shard_map/all_to_all | solution.py:73
  107.7 56.5 %all-gather.3.cloned.1.call-done = bf16[2048,2048]{1,0:T(8,128)(2,1)} async-done(((bf16[2048,128]{1,0:T(8,128)(2,1)}), bf16[2048,2048]{1,0:T(8,128)(2,1)}) %all-gather.3.cloned.1.call-update) | async-done | bytes 8388624 | tf_op jit(solution)/shard_map/all_gather | solution.py:48
  164.2 4.6 %fusion.21 = bf16[16,8,16,128]{3,1,2,0:T(8,128)(2,1)S(1)} fusion(bf16[2048,2048]{1,0:T(8,128)(2,1)} %all-gather.3.cloned.1.call-done, bf16[1,128,2048]{2,1,0:T(8,128)(2,1)S(1)} %copy-done), kind=kOutput, calls=%fused_computation.29 | convolution fusion | flops 1074003968 | bytes 9437184 | tf_op jit(solution)/shard_map/dot_general | solution.py:46
  169.0 0.9 copy.48
  169.9 11.1 %all-to-all-start = ((bf16[128,16,1,128]{3,0,2,1:T(8,128)(2,1)}), bf16[128,16,1,128]{3,0,2,1:T(8,128)(2,1)S(1)}, u32[]{:S(2)}, u32[]{:S(2)}) async-start(bf16[128,16,1,128]{3,0,2,1:T(8,128)(2,1)} %copy.48), calls=%async_computation | async-start | bytes 1048576 | tf_op jit(solution)/shard_map/all_to_all | solution.py:71
  182.2 0.8 dynamic_slice.21
  184.5 2.3 fusion.25
  186.9 23.1 %all-to-all-done = bf16[128,16,1,128]{3,0,2,1:T(8,128)(2,1)S(1)} async-done(((bf16[128,16,1,128]{3,0,2,1:T(8,128)(2,1)}), bf16[128,16,1,128]{3,0,2,1:T(8,128)(2,1)S(1)}, u32[]{:S(2)}, u32[]{:S(2)}) %all-to-all-start) | async-done | bytes 524320 | tf_op jit(solution)/shard_map/all_to_all | solution.py:71
  210.0 0.9 broadcast_in_dim.38
  210.9 6.8 %all-to-all-start.3 = ((bf16[128,16,1,128]{3,0,2,1:T(8,128)(2,1)}), bf16[128,16,1,128]{3,0,2,1:T(8,128)(2,1)S(1)}, u32[]{:S(2)}, u32[]{:S(2)}) async-start(bf16[128,16,1,128]{3,0,2,1:T(8,128)(2,1)} %bitcast.31), calls=%async_computation.3 | async-start | bytes 1048576 | tf_op jit(solution)/shard_map/all_to_all | solution.py:74
  219.8 26.8 %all-to-all-done.3 = bf16[128,16,1,128]{3,0,2,1:T(8,128)(2,1)S(1)} async-done(((bf16[128,16,1,128]{3,0,2,1:T(8,128)(2,1)}), bf16[128,16,1,128]{3,0,2,1:T(8,128)(2,1)S(1)}, u32[]{:S(2)}, u32[]{:S(2)}) %all-to-all-start.3) | async-done | bytes 524320 | tf_op jit(solution)/shard_map/all_to_all | solution.py:74
  246.6 19.9 %while.11 = (s32[]{:T(128)}, bf16[4,512,1,1,128]{4,1,0,3,2:T(8,128)(2,1)S(1)}, s32[4]{0:T(128)S(1)}, bf16[2048,1,1,128]{3,0,2,1:T(8,128)(2,1)S(1)}, bf16[2048,1,...) while((s32[]{:T(128)}, ...), condition=%wide.region_8.9_spmd.clone, body=%wide.region_4.8_spmd.clone.sunk | while | flops 548732928 | bytes 14979803 | solution.py:120
  247.9 1.3 fusion.41
  249.2 0.7 fusion.42
  249.9 1.4 multiply_reduce_fusion.4
  252.9 1.3 fusion.41
  254.9 1.4 multiply_reduce_fusion.4
  257.9 1.3 fusion.41
  259.1 0.7 fusion.42
  259.9 1.4 multiply_reduce_fusion.4
  262.9 1.3 fusion.41
  264.8 1.4 multiply_reduce_fusion.4
  267.1 1.0 reduce.14
  268.2 35.4 %all_to_all.57 = bf16[16,2,8192]{2,1,0:T(2,128)(2,1)S(1)} all-to-all(bf16[16,2,8192]{2,1,0:T(2,128)(2,1)S(1)} %reshape.438), channel_id=1, replica_groups=mesh['grp'=2,'sp'=16,'dp'=16] {'sp'}, dimensions={0} | all-to-all | bytes 1048576 | tf_op jit(solution)/shard_map/all_to_all | solution.py:122
  304.5 1.0 copy.57
  (71 shorter events, 11.5 us)
Async XLA Ops:
  6.5 2.6 copy-start
  6.6 84.7 %all-gather.5.cloned.1.call-start = ((), (), s32[]{:S(2)}) async-start(), calls=%async_computation.6 | async-start | bytes 4456448 | tf_op jit(solution)/shard_map/all_gather | solution.py:14
  8.4 155.8 %all-gather.3.cloned.1.call-start = ((), (), s32[]{:S(2)}) async-start(), calls=%async_computation.5 | async-start | bytes 8912896 | tf_op jit(solution)/shard_map/all_gather | solution.py:48
  10.9 82.8 %all-to-all-start.2 = ((bf16[128,16,1]{0,2,1:T(2,128)(2,1)}), bf16[128,16,1]{0,2,1:T(2,128)(2,1)S(1)}, u32[]{:S(2)}, u32[]{:S(2)}) async-start(bf16[128,16,1]{0,2,1:T(2,128)(2,1)} %copy.52), calls=%async_computation.2 | async-start | bytes 16384 | tf_op jit(solution)/shard_map/all_to_all | solution.py:72
  94.6 75.3 %all-to-all-start.1 = ((bf16[128,16,1,128]{3,0,2,1:T(8,128)(2,1)}), bf16[128,16,1,128]{3,0,2,1:T(8,128)(2,1)S(1)}, u32[]{:S(2)}, u32[]{:S(2)}) async-start(bf16[128,16,1,128]{3,0,2,1:T(8,128)(2,1)} %bitcast.10), calls=%async_computation.1 | async-start | bytes 1048576 | tf_op jit(solution)/shard_map/all_to_all | solution.py:73
  107.7 73.3 %copy-start.1 = (f32[16]{0:T(128)S(1)}, f32[16]{0:T(128)}, u32[]{:S(2)}) copy-start(f32[16]{0:T(128)} %param.18) | copy-start | bytes 196
  107.7 73.9 %copy-start.2 = (f32[16]{0:T(128)S(1)}, f32[16]{0:T(128)}, u32[]{:S(2)}) copy-start(f32[16]{0:T(128)} %param.17) | copy-start | bytes 196
  169.9 40.1 %all-to-all-start = ((bf16[128,16,1,128]{3,0,2,1:T(8,128)(2,1)}), bf16[128,16,1,128]{3,0,2,1:T(8,128)(2,1)S(1)}, u32[]{:S(2)}, u32[]{:S(2)}) async-start(bf16[128,16,1,128]{3,0,2,1:T(8,128)(2,1)} %copy.48), calls=%async_computation | async-start | bytes 1048576 | tf_op jit(solution)/shard_map/all_to_all | solution.py:71
  210.9 35.7 %all-to-all-start.3 = ((bf16[128,16,1,128]{3,0,2,1:T(8,128)(2,1)}), bf16[128,16,1,128]{3,0,2,1:T(8,128)(2,1)S(1)}, u32[]{:S(2)}, u32[]{:S(2)}) async-start(bf16[128,16,1,128]{3,0,2,1:T(8,128)(2,1)} %bitcast.31), calls=%async_computation.3 | async-start | bytes 1048576 | tf_op jit(solution)/shard_map/all_to_all | solution.py:74
Sparse Core Ops, SparseCore 0:
  9.5 81.7 all-gather.4
  93.3 70.8 all-gather.2
where the time goes:
time: 313 us; the launch traced here: 312 us
  waiting for transfers between devices  144 us (46%)
  starting transfers between devices  74.7 us (24%)
  blocking collectives  35.4 us (11%)
  matrix products  21.2 us (7%)
  between operations  14.3 us (5%)
  local copies, waits for them, and re-layouts  11.5 us (4%)
  other arithmetic  8.64 us (3%)
    all_gather x1, waiting for transfers between devices, local(): lax.all_gather(q_weight, 'dp', axis=1, tiled=True)  56.5 us
    all_to_all x1, starting transfers between devices, local(): lax.all_to_all(forget_send, 'sp', split_axis=1, concat_axis=0, tiled=True)  43.7 us
    all_gather x1, waiting for transfers between devices, turned_gather(): whole, at, done = (lax.all_gather(both, axis, axis=0, tiled=True), 0, [])  36.7 us
    all_to_all x1, blocking collectives, local(): lax.all_to_all(outputs, 'sp', split_axis=0, concat_axis=1, tiled=True)  35.4 us
    all_to_all x1, waiting for transfers between devices, local(): lax.all_to_all(value_send, 'sp', split_axis=1, concat_axis=0, tiled=True)  26.8 us
    all_to_all x1, waiting for transfers between devices, local(): lax.all_to_all(query_send, 'sp', split_axis=1, concat_axis=0, tiled=True)  23.1 us
    all_to_all x1, starting transfers between devices, local(): lax.all_to_all(key_send, 'sp', split_axis=1, concat_axis=0, tiled=True)  13.1 us
    all_to_all x1, starting transfers between devices, local(): lax.all_to_all(query_send, 'sp', split_axis=1, concat_axis=0, tiled=True)  11.1 us
  transfers between devices with their start and end apart: 6, of which 4 were waited for; matrix products, arithmetic and copies ran while one was open for 6% of the time, Pallas kernels for 0%

commit v1 on v0

--- a/solution.py
+++ b/solution.py
@@ -2,10 +2,18 @@
 import jax.numpy as jnp
 from jax import lax
 from jax.sharding import PartitionSpec as P
+from jax.lax import axis_index, axis_size, ppermute
 
 NEG = -1e30
 QK_FLOOR = 0.1
 OUT_FLOOR = 0.001
+
+
+def numbers_keep_up(x_local, where_dim):
+    r2 = list(x_local.shape[1:])
+    r2[where_dim] *= x_local.shape[0]
+    left_arr = jnp.moveaxis(x_local, 0, where_dim).reshape(r2)
+    return left_arr
 
 
 def turned_gather(arrays, axis, dims):
@@ -43,10 +51,25 @@
     local_heads = head_count // spread
     local_kv = max(1, kv_heads // spread)
     group_size = local_heads // local_kv
+
+    def task_number(page, net_axis, out_dim):
+        dev_n = axis_size(net_axis)
+        made = tuple(((dev_j, (dev_j + 1) % dev_n) for dev_j in range(dev_n)))
+        windows = tuple(((dev, idx) for idx, dev in made))
+        parts_out, m_next = ([], [])
+        for pp in range(dev_n - 1):
+            if pp % 2 == 0:
+                parts_out.append(ppermute(parts_out[-1] if parts_out else page, net_axis, made))
+            else:
+                m_next.append(ppermute(m_next[-1] if m_next else page, net_axis, windows))
+        outcome_arr = jnp.stack([*parts_out[::-1], page, *m_next], axis=0)
+        z = axis_index(net_axis) - len(parts_out)
+        outcome_arr = outcome_arr[(jnp.arange(dev_n) - z) % dev_n]
+        block_next = numbers_keep_up(outcome_arr, out_dim)
+        return block_next
+
     queries = jnp.dot(
-        own_rows,
-        lax.all_gather(q_weight, "dp", axis=1, tiled=True),
-        preferred_element_type=jnp.float32,
+        own_rows, task_number(q_weight, "dp", 1), preferred_element_type=jnp.float32
     ).astype(jnp.bfloat16)
     key_full, value_full = turned_gather((k_weight, v_weight), "dp", (1, 1))
     keys_proj = jnp.dot(own_rows, key_full, preferred_element_type=jnp.float32).astype(jnp.bfloat16)

time: 313 us -> 356 us (1.14)
  the two profiles are of different devices: /device:TPU:66 before, /device:TPU:86 now
where the time goes in v1:
time: 356 us; the launch traced here: 354 us
  waiting for transfers between devices  107 us (30%)
  starting transfers between devices  104 us (29%)
  local copies, waits for them, and re-layouts  57.9 us (16%)
  blocking collectives  35.4 us (10%)
  matrix products  23.1 us (6%)
  between operations  14.4 us (4%)
  other arithmetic  9.6 us (3%)
    all_to_all x1, starting transfers between devices, local(): lax.all_to_all(forget_send, 'sp', split_axis=1, concat_axis=0, tiled=True)  43.7 us
    all_to_all x1, blocking collectives, local(): lax.all_to_all(outputs, 'sp', split_axis=0, concat_axis=1, tiled=True)  35.4 us
    ppermute x8, waiting for transfers between devices, task_number(): ppermute(parts_out[-1] if parts_out else page, net_axis, made)  35.2 us
    all_to_all x1, waiting for transfers between devices, local(): lax.all_to_all(value_send, 'sp', split_axis=1, concat_axis=0, tiled=True)  26.7 us
    ppermute x8, starting transfers between devices, task_number(): ppermute(parts_out[-1] if parts_out else page, net_axis, made)  24.6 us
    all_to_all x1, waiting for transfers between devices, local(): lax.all_to_all(key_send, 'sp', split_axis=1, concat_axis=0, tiled=True)  23.4 us
    unnamed x36, local copies, waits for them, and re-layouts  23.4 us
    all_to_all x1, waiting for transfers between devices, local(): lax.all_to_all(query_send, 'sp', split_axis=1, concat_axis=0, tiled=True)  20.5 us
  transfers between devices with their start and end apart: 20, of which 11 were waited for; matrix products, arithmetic and copies ran while one was open for 18% of the time, Pallas kernels for 0%

profile of v1, /device:TPU:86, one launch (start us, length us, event | category | flops | bytes accessed | tf_op | source)
XLA Modules:
  0.0 354.1 jit_solution(16044894735676828040)
XLA Ops:
  6.6 8.8 %collective-permute-done = bf16[2048,128]{1,0:T(8,128)(2,1)S(1)} collective-permute-done((bf16[2048,128]{1,0:T(8,128)(2,1)}, bf16[2048,128]{1,0:T(8,128)(2,1)S(1)}, u32[]{:S(2)}, u32[]{:S(2)}) %collective-permute-start) | collective-permute-done | bytes 524320 | tf_op jit(solution)/shard_map/ppermute | solution.py:62
  17.1 6.9 %collective-permute-done.1 = bf16[2048,128]{1,0:T(8,128)(2,1)S(1)} collective-permute-done((bf16[2048,128]{1,0:T(8,128)(2,1)S(1)}, bf16[2048,128]{1,0:T(8,128)(2,1)S(1)}, u32[]{:S(2)}, u32[]{:S(2)}) %collective-permute-start.1) | collective-permute-done | bytes 524320 | tf_op jit(solution)/shard_map/ppermute | solution.py:62
  25.9 6.6 %collective-permute-done.2 = bf16[2048,128]{1,0:T(8,128)(2,1)S(1)} collective-permute-done((bf16[2048,128]{1,0:T(8,128)(2,1)S(1)}, bf16[2048,128]{1,0:T(8,128)(2,1)S(1)}, u32[]{:S(2)}, u32[]{:S(2)}) %collective-permute-start.2) | collective-permute-done | bytes 524320 | tf_op jit(solution)/shard_map/ppermute | solution.py:62
  32.6 2.9 collective-permute-start.3
  35.5 5.7 %collective-permute-done.3 = bf16[2048,128]{1,0:T(8,128)(2,1)S(1)} collective-permute-done((bf16[2048,128]{1,0:T(8,128)(2,1)S(1)}, bf16[2048,128]{1,0:T(8,128)(2,1)S(1)}, u32[]{:S(2)}, u32[]{:S(2)}) %collective-permute-start.3) | collective-permute-done | bytes 524320 | tf_op jit(solution)/shard_map/ppermute | solution.py:62
  41.2 4.1 %collective-permute-start.4 = (bf16[2048,128]{1,0:T(8,128)(2,1)S(1)}, bf16[2048,128]{1,0:T(8,128)(2,1)S(1)}, u32[]{:S(2)}, u32[]{:S(2)}) collective-permute-start(bf16[2048,128]{1,0:T(8,128)(2,1)S(1)} %collective-permute-done.3), channel_id=1, source_target_pairs={{0,1},{1,2},{2,3},{3,4},{4,5},{5,6},{6,7},{7,8},{8,9},{9,10},{10,1... | collective-permute-start | bytes 1572872 | tf_op jit(solution)/shard_map/ppermute | solution.py:62
  46.1 3.7 %collective-permute-done.4 = bf16[2048,128]{1,0:T(8,128)(2,1)S(1)} collective-permute-done((bf16[2048,128]{1,0:T(8,128)(2,1)S(1)}, bf16[2048,128]{1,0:T(8,128)(2,1)S(1)}, u32[]{:S(2)}, u32[]{:S(2)}) %collective-permute-start.4) | collective-permute-done | bytes 524320 | tf_op jit(solution)/shard_map/ppermute | solution.py:62
  49.8 5.3 %collective-permute-start.5 = (bf16[2048,128]{1,0:T(8,128)(2,1)S(1)}, bf16[2048,128]{1,0:T(8,128)(2,1)}, u32[]{:S(2)}, u32[]{:S(2)}) collective-permute-start(bf16[2048,128]{1,0:T(8,128)(2,1)S(1)} %collective-permute-done.4), channel_id=1, source_target_pairs={{0,1},{1,2},{2,3},{3,4},{4,5},{5,6},{6,7},{7,8},{8,9},{9,10},{10,1... | collective-permute-start | bytes 1572872 | tf_op jit(solution)/shard_map/ppermute | solution.py:62
  55.1 3.4 collective-permute-done.5
  58.5 6.4 %collective-permute-start.6 = (bf16[2048,128]{1,0:T(8,128)(2,1)}, bf16[2048,128]{1,0:T(8,128)(2,1)}, u32[]{:S(2)}, u32[]{:S(2)}) collective-permute-start(bf16[2048,128]{1,0:T(8,128)(2,1)} %collective-permute-done.5), channel_id=1, source_target_pairs={{0,1},{1,2},{2,3},{3,4},{4,5},{5,6},{6,7},{7,8},{8,9},{9,10},{10,1... | collective-permute-start | bytes 1572872 | tf_op jit(solution)/shard_map/ppermute | solution.py:62
  66.6 43.7 %all-to-all-start.2 = ((bf16[128,16,1]{0,2,1:T(2,128)(2,1)}), bf16[128,16,1]{0,2,1:T(2,128)(2,1)S(1)}, u32[]{:S(2)}, u32[]{:S(2)}) async-start(bf16[128,16,1]{0,2,1:T(2,128)(2,1)} %copy.37), calls=%async_computation.2 | async-start | bytes 16384 | tf_op jit(solution)/shard_map/all_to_all | solution.py:95
  110.5 3.6 %collective-permute-start.7 = (bf16[2048,128]{1,0:T(8,128)(2,1)}, bf16[2048,128]{1,0:T(8,128)(2,1)}, u32[]{:S(2)}, u32[]{:S(2)}) collective-permute-start(bf16[2048,128]{1,0:T(8,128)(2,1)} %collective-permute-done.6), channel_id=1, source_target_pairs={{0,1},{1,2},{2,3},{3,4},{4,5},{5,6},{6,7},{7,8},{8,9},{9,10},{10,1... | collective-permute-start | bytes 1572872 | tf_op jit(solution)/shard_map/ppermute | solution.py:62
  117.5 1.9 collective-permute-start.14
  123.2 1.9 bitcast_dynamic-update-slice_fusion.13
  128.8 1.9 bitcast_dynamic-update-slice_fusion.10
  135.7 1.9 bitcast_dynamic-update-slice_fusion.3
  137.6 1.9 bitcast_dynamic-update-slice_fusion.2
  139.5 1.9 bitcast_dynamic-update-slice_fusion.1
  142.3 8.4 %gather_fusion = bf16[16,2048,128]{2,1,0:T(8,128)(2,1)} fusion(bf16[16,2048,128]{2,1,0:T(8,128)(2,1)} %bitcast_dynamic-update-slice_fusion, s32[1024]{0:T(1024)S(1)} %pad_clamp_fusion), kind=kCustom, calls=%fused_computation | custom fusion | bytes 16777280 | tf_op jit(solution)/shard_map/gather | solution.py:67
  150.6 12.4 %copy.33 = bf16[2048,16,128]{0,2,1:T(8,128)(2,1)} copy(bf16[2048,16,128]{2,0,1:T(8,128)(2,1)} %bitcast.175) | data formatting | bytes 16777216 | tf_op jit(solution)/shard_map/transpose | solution.py:15
  163.0 6.6 %convolution_convert_fusion = bf16[2048,128]{1,0:T(8,128)(2,1)} fusion(bf16[2048,2048]{0,1:T(8,128)(2,1)} %bitcast.176, bf16[1,128,2048]{2,1,0:T(8,128)(2,1)S(1)} %copy-done), kind=kOutput, calls=%fused_computation.25 | convolution fusion | flops 1074003968 | bytes 9437184 | tf_op jit(solution)/shard_map/dot_general | solution.py:71
  169.6 12.0 %all-to-all-start = ((bf16[128,16,1,128]{0,3,2,1:T(8,128)(2,1)}), bf16[128,16,1,128]{0,3,2,1:T(8,128)(2,1)S(1)}, u32[]{:S(2)}, u32[]{:S(2)}) async-start(bf16[128,16,1,128]{0,3,2,1:T(8,128)(2,1)} %bitcast.22), calls=%async_computation | async-start | bytes 1048576 | tf_op jit(solution)/shard_map/all_to_all | solution.py:94
  181.7 2.3 fusion.21
  184.1 20.5 %all-to-all-done = bf16[128,16,1,128]{0,3,2,1:T(8,128)(2,1)S(1)} async-done(((bf16[128,16,1,128]{0,3,2,1:T(8,128)(2,1)}), bf16[128,16,1,128]{0,3,2,1:T(8,128)(2,1)S(1)}, u32[]{:S(2)}, u32[]{:S(2)}) %all-to-all-start) | async-done | bytes 524320 | tf_op jit(solution)/shard_map/all_to_all | solution.py:94
  205.5 12.9 %all-to-all-start.1 = ((bf16[128,16,1,128]{3,0,2,1:T(8,128)(2,1)}), bf16[128,16,1,128]{3,0,2,1:T(8,128)(2,1)S(1)}, u32[]{:S(2)}, u32[]{:S(2)}) async-start(bf16[128,16,1,128]{3,0,2,1:T(8,128)(2,1)} %bitcast.32), calls=%async_computation.1 | async-start | bytes 1048576 | tf_op jit(solution)/shard_map/all_to_all | solution.py:96
  222.0 2.3 fusion.24
  224.5 23.4 %all-to-all-done.1 = bf16[128,16,1,128]{3,0,2,1:T(8,128)(2,1)S(1)} async-done(((bf16[128,16,1,128]{3,0,2,1:T(8,128)(2,1)}), bf16[128,16,1,128]{3,0,2,1:T(8,128)(2,1)S(1)}, u32[]{:S(2)}, u32[]{:S(2)}) %all-to-all-start.1) | async-done | bytes 524320 | tf_op jit(solution)/shard_map/all_to_all | solution.py:96
  248.8 6.9 %all-to-all-start.3 = ((bf16[128,16,1,128]{3,0,2,1:T(8,128)(2,1)}), bf16[128,16,1,128]{3,0,2,1:T(8,128)(2,1)S(1)}, u32[]{:S(2)}, u32[]{:S(2)}) async-start(bf16[128,16,1,128]{3,0,2,1:T(8,128)(2,1)} %bitcast.53), calls=%async_computation.3 | async-start | bytes 1048576 | tf_op jit(solution)/shard_map/all_to_all | solution.py:97
  258.0 26.7 %all-to-all-done.3 = bf16[128,16,1,128]{3,0,2,1:T(8,128)(2,1)S(1)} async-done(((bf16[128,16,1,128]{3,0,2,1:T(8,128)(2,1)}), bf16[128,16,1,128]{3,0,2,1:T(8,128)(2,1)S(1)}, u32[]{:S(2)}, u32[]{:S(2)}) %all-to-all-start.3) | async-done | bytes 524320 | tf_op jit(solution)/shard_map/all_to_all | solution.py:97
  284.6 22.6 %while.11 = (s32[]{:T(128)}, bf16[4,512,1,1,128]{4,1,0,3,2:T(8,128)(2,1)}, s32[4]{0:T(128)S(1)}, bf16[2048,1,1,128]{3,0,2,1:T(8,128)(2,1)S(1)}, bf16[2048,1,128]...) while((s32[]{:T(128)}, ...), condition=%wide.region_8.9_spmd.clone, body=%wide.region_4.8_spmd.clone.sunk | while | flops 548732928 | bytes 14980303 | solution.py:143
  307.8 2.0 reduce.14
  309.9 35.4 %all_to_all.57 = bf16[16,2,8192]{2,1,0:T(2,128)(2,1)S(1)} all-to-all(bf16[16,2,8192]{2,1,0:T(2,128)(2,1)S(1)} %reshape.499), channel_id=1, replica_groups=mesh['grp'=2,'sp'=16,'dp'=16] {'sp'}, dimensions={0} | all-to-all | bytes 1048576 | tf_op jit(solution)/shard_map/all_to_all | solution.py:145
  (128 shorter events, 52.9 us)
Async XLA Ops:
  6.5 58.4 %copy-start = (bf16[1,128,2048]{2,1,0:T(8,128)(2,1)S(1)}, bf16[1,128,2048]{2,1,0:T(8,128)(2,1)}, u32[]{:S(2)}) copy-start(bf16[1,128,2048]{2,1,0:T(8,128)(2,1)} %param.11) | copy-start | bytes 1572868
  6.6 125.8 %copy-start.1 = (bf16[2048,128]{1,0:T(8,128)(2,1)S(1)}, bf16[2048,128]{1,0:T(8,128)(2,1)}, u32[]{:S(2)}) copy-start(bf16[2048,128]{1,0:T(8,128)(2,1)} %param.13) | copy-start | bytes 1572868
  6.6 8.8 %collective-permute-start = (bf16[2048,128]{1,0:T(8,128)(2,1)}, bf16[2048,128]{1,0:T(8,128)(2,1)S(1)}, u32[]{:S(2)}, u32[]{:S(2)}) collective-permute-start(bf16[2048,128]{1,0:T(8,128)(2,1)} %param.13), channel_id=1, source_target_pairs={{0,1},{1,2},{2,3},{3,4},{4,5},{5,6},{6,7},{7,8},{8,9},{9,10},{10,1... | collective-permute-start | bytes 1572872 | tf_op jit(solution)/shard_map/ppermute | solution.py:62
  15.4 8.6 %collective-permute-start.1 = (bf16[2048,128]{1,0:T(8,128)(2,1)S(1)}, bf16[2048,128]{1,0:T(8,128)(2,1)S(1)}, u32[]{:S(2)}, u32[]{:S(2)}) collective-permute-start(bf16[2048,128]{1,0:T(8,128)(2,1)S(1)} %collective-permute-done), channel_id=1, source_target_pairs={{0,1},{1,2},{2,3},{3,4},{4,5},{5,6},{6,7},{7,8},{8,9},{9,10},{10,1... | collective-permute-start | bytes 1572872 | tf_op jit(solution)/shard_map/ppermute | solution.py:62
  15.9 9.7 %collective-permute-start.8 = (bf16[2048,128]{1,0:T(8,128)(2,1)}, bf16[2048,128]{1,0:T(8,128)(2,1)S(1)}, u32[]{:S(2)}, u32[]{:S(2)}) collective-permute-start(bf16[2048,128]{1,0:T(8,128)(2,1)} %param.13), channel_id=1, source_target_pairs={{1,0},{2,1},{3,2},{4,3},{5,4},{6,5},{7,6},{8,7},{9,8},{10,9},{11,1... | collective-permute-start | bytes 1572872 | tf_op jit(solution)/shard_map/ppermute | solution.py:64
  24.0 8.6 %collective-permute-start.2 = (bf16[2048,128]{1,0:T(8,128)(2,1)S(1)}, bf16[2048,128]{1,0:T(8,128)(2,1)S(1)}, u32[]{:S(2)}, u32[]{:S(2)}) collective-permute-start(bf16[2048,128]{1,0:T(8,128)(2,1)S(1)} %collective-permute-done.1), channel_id=1, source_target_pairs={{0,1},{1,2},{2,3},{3,4},{4,5},{5,6},{6,7},{7,8},{8,9},{9,10},{10,1... | collective-permute-start | bytes 1572872 | tf_op jit(solution)/shard_map/ppermute | solution.py:62
  25.7 9.8 %collective-permute-start.9 = (bf16[2048,128]{1,0:T(8,128)(2,1)S(1)}, bf16[2048,128]{1,0:T(8,128)(2,1)S(1)}, u32[]{:S(2)}, u32[]{:S(2)}) collective-permute-start(bf16[2048,128]{1,0:T(8,128)(2,1)S(1)} %collective-permute-done.8), channel_id=1, source_target_pairs={{1,0},{2,1},{3,2},{4,3},{5,4},{6,5},{7,6},{8,7},{9,8},{10,9},{11,1... | collective-permute-start | bytes 1572872 | tf_op jit(solution)/shard_map/ppermute | solution.py:64
  32.6 12.7 %copy-start.2 = (bf16[2048,128]{1,0:T(8,128)(2,1)}, bf16[2048,128]{1,0:T(8,128)(2,1)S(1)}, u32[]{:S(2)}) copy-start(bf16[2048,128]{1,0:T(8,128)(2,1)S(1)} %collective-permute-done.2) | copy-start | bytes 1572868
  32.6 8.6 %collective-permute-start.3 = (bf16[2048,128]{1,0:T(8,128)(2,1)S(1)}, bf16[2048,128]{1,0:T(8,128)(2,1)S(1)}, u32[]{:S(2)}, u32[]{:S(2)}) collective-permute-start(bf16[2048,128]{1,0:T(8,128)(2,1)S(1)} %collective-permute-done.2), channel_id=1, source_target_pairs={{0,1},{1,2},{2,3},{3,4},{4,5},{5,6},{6,7},{7,8},{8,9},{9,10},{10,1... | collective-permute-start | bytes 1572872 | tf_op jit(solution)/shard_map/ppermute | solution.py:62
  35.5 9.8 %collective-permute-start.10 = (bf16[2048,128]{1,0:T(8,128)(2,1)S(1)}, bf16[2048,128]{1,0:T(8,128)(2,1)S(1)}, u32[]{:S(2)}, u32[]{:S(2)}) collective-permute-start(bf16[2048,128]{1,0:T(8,128)(2,1)S(1)} %collective-permute-done.9), channel_id=1, source_target_pairs={{1,0},{2,1},{3,2},{4,3},{5,4},{6,5},{7,6},{8,7},{9,8},{10,9},{11,1... | collective-permute-start | bytes 1572872 | tf_op jit(solution)/shard_map/ppermute | solution.py:64
  41.2 13.9 %copy-start.5 = (bf16[2048,128]{1,0:T(8,128)(2,1)}, bf16[2048,128]{1,0:T(8,128)(2,1)S(1)}, u32[]{:S(2)}) copy-start(bf16[2048,128]{1,0:T(8,128)(2,1)S(1)} %collective-permute-done.3) | copy-start | bytes 1572868
  41.2 8.6 %collective-permute-start.4 = (bf16[2048,128]{1,0:T(8,128)(2,1)S(1)}, bf16[2048,128]{1,0:T(8,128)(2,1)S(1)}, u32[]{:S(2)}, u32[]{:S(2)}) collective-permute-start(bf16[2048,128]{1,0:T(8,128)(2,1)S(1)} %collective-permute-done.3), channel_id=1, source_target_pairs={{0,1},{1,2},{2,3},{3,4},{4,5},{5,6},{6,7},{7,8},{8,9},{9,10},{10,1... | collective-permute-start | bytes 1572872 | tf_op jit(solution)/shard_map/ppermute | solution.py:62
  45.3 0.8 copy-start.3
  45.3 9.8 %collective-permute-start.11 = (bf16[2048,128]{1,0:T(8,128)(2,1)S(1)}, bf16[2048,128]{1,0:T(8,128)(2,1)}, u32[]{:S(2)}, u32[]{:S(2)}) collective-permute-start(bf16[2048,128]{1,0:T(8,128)(2,1)S(1)} %collective-permute-done.10), channel_id=1, source_target_pairs={{1,0},{2,1},{3,2},{4,3},{5,4},{6,5},{7,6},{8,7},{9,8},{10,9},{11,1... | collective-permute-start | bytes 1572872 | tf_op jit(solution)/shard_map/ppermute | solution.py:64
  49.8 5.3 %copy-start.6 = (bf16[2048,128]{1,0:T(8,128)(2,1)}, bf16[2048,128]{1,0:T(8,128)(2,1)S(1)}, u32[]{:S(2)}) copy-start(bf16[2048,128]{1,0:T(8,128)(2,1)S(1)} %collective-permute-done.4) | copy-start | bytes 1572868
  49.8 8.7 %collective-permute-start.5 = (bf16[2048,128]{1,0:T(8,128)(2,1)S(1)}, bf16[2048,128]{1,0:T(8,128)(2,1)}, u32[]{:S(2)}, u32[]{:S(2)}) collective-permute-start(bf16[2048,128]{1,0:T(8,128)(2,1)S(1)} %collective-permute-done.4), channel_id=1, source_target_pairs={{0,1},{1,2},{2,3},{3,4},{4,5},{5,6},{6,7},{7,8},{8,9},{9,10},{10,1... | collective-permute-start | bytes 1572872 | tf_op jit(solution)/shard_map/ppermute | solution.py:62
  55.1 55.3 %collective-permute-start.12 = (bf16[2048,128]{1,0:T(8,128)(2,1)}, bf16[2048,128]{1,0:T(8,128)(2,1)}, u32[]{:S(2)}, u32[]{:S(2)}) collective-permute-start(bf16[2048,128]{1,0:T(8,128)(2,1)} %collective-permute-done.11), channel_id=1, source_target_pairs={{1,0},{2,1},{3,2},{4,3},{5,4},{6,5},{7,6},{8,7},{9,8},{10,9},{11,1... | collective-permute-start | bytes 1572872 | tf_op jit(solution)/shard_map/ppermute | solution.py:64
  58.5 52.0 %collective-permute-start.6 = (bf16[2048,128]{1,0:T(8,128)(2,1)}, bf16[2048,128]{1,0:T(8,128)(2,1)}, u32[]{:S(2)}, u32[]{:S(2)}) collective-permute-start(bf16[2048,128]{1,0:T(8,128)(2,1)} %collective-permute-done.5), channel_id=1, source_target_pairs={{0,1},{1,2},{2,3},{3,4},{4,5},{5,6},{6,7},{7,8},{8,9},{9,10},{10,1... | collective-permute-start | bytes 1572872 | tf_op jit(solution)/shard_map/ppermute | solution.py:62
  66.6 103.0 %all-to-all-start.2 = ((bf16[128,16,1]{0,2,1:T(2,128)(2,1)}), bf16[128,16,1]{0,2,1:T(2,128)(2,1)S(1)}, u32[]{:S(2)}, u32[]{:S(2)}) async-start(bf16[128,16,1]{0,2,1:T(2,128)(2,1)} %copy.37), calls=%async_computation.2 | async-start | bytes 16384 | tf_op jit(solution)/shard_map/all_to_all | solution.py:95
  110.3 71.3 %all-gather.2.cloned.1.call-start = ((), (), s32[]{:S(2)}) async-start(), calls=%async_computation.5 | async-start | bytes 4456448 | tf_op jit(solution)/shard_map/all_gather | solution.py:22
  110.4 7.1 %collective-permute-start.13 = (bf16[2048,128]{1,0:T(8,128)(2,1)}, bf16[2048,128]{1,0:T(8,128)(2,1)}, u32[]{:S(2)}, u32[]{:S(2)}) collective-permute-start(bf16[2048,128]{1,0:T(8,128)(2,1)} %collective-permute-done.12), channel_id=1, source_target_pairs={{1,0},{2,1},{3,2},{4,3},{5,4},{6,5},{7,6},{8,7},{9,8},{10,9},{11,1... | collective-permute-start | bytes 1572872 | tf_op jit(solution)/shard_map/ppermute | solution.py:64
  110.5 9.0 %collective-permute-start.7 = (bf16[2048,128]{1,0:T(8,128)(2,1)}, bf16[2048,128]{1,0:T(8,128)(2,1)}, u32[]{:S(2)}, u32[]{:S(2)}) collective-permute-start(bf16[2048,128]{1,0:T(8,128)(2,1)} %collective-permute-done.6), channel_id=1, source_target_pairs={{0,1},{1,2},{2,3},{3,4},{4,5},{5,6},{6,7},{7,8},{8,9},{9,10},{10,1... | collective-permute-start | bytes 1572872 | tf_op jit(solution)/shard_map/ppermute | solution.py:62
  115.8 19.1 %copy-start.4 = (bf16[2048,128]{1,0:T(8,128)(2,1)S(1)}, bf16[2048,128]{1,0:T(8,128)(2,1)}, u32[]{:S(2)}) copy-start(bf16[2048,128]{1,0:T(8,128)(2,1)} %copy-done.3) | copy-start | bytes 1572868
  117.5 23.9 %collective-permute-start.14 = (bf16[2048,128]{1,0:T(8,128)(2,1)}, bf16[2048,128]{1,0:T(8,128)(2,1)S(1)}, u32[]{:S(2)}, u32[]{:S(2)}) collective-permute-start(bf16[2048,128]{1,0:T(8,128)(2,1)} %collective-permute-done.13), channel_id=1, source_target_pairs={{1,0},{2,1},{3,2},{4,3},{5,4},{6,5},{7,6},{8,7},{9,8},{10,9},{11,1... | collective-permute-start | bytes 1572872 | tf_op jit(solution)/shard_map/ppermute | solution.py:64
  163.0 55.3 %copy-start.7 = (f32[16]{0:T(128)S(1)}, f32[16]{0:T(128)}, u32[]{:S(2)}) copy-start(f32[16]{0:T(128)} %param.17) | copy-start | bytes 196
  163.0 55.9 %copy-start.8 = (f32[16]{0:T(128)S(1)}, f32[16]{0:T(128)}, u32[]{:S(2)}) copy-start(f32[16]{0:T(128)} %param.18) | copy-start | bytes 196
  169.6 35.0 %all-to-all-start = ((bf16[128,16,1,128]{0,3,2,1:T(8,128)(2,1)}), bf16[128,16,1,128]{0,3,2,1:T(8,128)(2,1)S(1)}, u32[]{:S(2)}, u32[]{:S(2)}) async-start(bf16[128,16,1,128]{0,3,2,1:T(8,128)(2,1)} %bitcast.22), calls=%async_computation | async-start | bytes 1048576 | tf_op jit(solution)/shard_map/all_to_all | solution.py:94
  205.5 42.4 %all-to-all-start.1 = ((bf16[128,16,1,128]{3,0,2,1:T(8,128)(2,1)}), bf16[128,16,1,128]{3,0,2,1:T(8,128)(2,1)S(1)}, u32[]{:S(2)}, u32[]{:S(2)}) async-start(bf16[128,16,1,128]{3,0,2,1:T(8,128)(2,1)} %bitcast.32), calls=%async_computation.1 | async-start | bytes 1048576 | tf_op jit(solution)/shard_map/all_to_all | solution.py:96
  248.8 35.8 %all-to-all-start.3 = ((bf16[128,16,1,128]{3,0,2,1:T(8,128)(2,1)}), bf16[128,16,1,128]{3,0,2,1:T(8,128)(2,1)S(1)}, u32[]{:S(2)}, u32[]{:S(2)}) async-start(bf16[128,16,1,128]{3,0,2,1:T(8,128)(2,1)} %bitcast.53), calls=%async_computation.3 | async-start | bytes 1048576 | tf_op jit(solution)/shard_map/all_to_all | solution.py:97
Sparse Core Ops, SparseCore 0:
  115.9 48.1 all-gather.1
